TPU v7x, 512 devices: a whole 4x8x8 slice. The times are simulated.
512 devices in a mesh: sp: 64 (over z, y), tp: 4 (over x), dp: 2 (over core).
Axes of the slice: x: 4, y: 8, z: 8, core: 2. Of those that a mesh axis runs over, the one named last changes fastest.
Arguments:
- latent: bfloat16 [2, 16384, 2048], P('dp', 'sp'), may hold values from -1.5 to 1.5
- condition: bfloat16 [2, 2048], P('dp', 'sp'), may hold values from -6 to 6
- context: bfloat16 [2, 1024, 2048], P('dp', 'sp'), may hold values from -6 to 6
- context_code: bfloat16 [2048], P('sp'), may hold values from -6 to 6
- shift_weight: bfloat16 [2048, 2048], P('sp', 'tp'), may hold values from -0.125 to 0.125
- scale_weight: bfloat16 [2048, 2048], P('sp', 'tp'), may hold values from -0.125 to 0.125
- gate_weight: bfloat16 [2048, 2048], P('sp', 'tp'), may hold values from -0.125 to 0.125
- norm_gain: float32 [2048], replicated, may hold values from 0.1 to 1.9
- query_weight: bfloat16 [2048, 1024], P(None, 'tp'), may hold values from -0.125 to 0.125
- key_weight: bfloat16 [2048, 256], P(None, 'tp'), may hold values from -0.125 to 0.125
- value_weight: bfloat16 [2048, 256], P(None, 'tp'), may hold values from -0.125 to 0.125
- output_weight: bfloat16 [1024, 2048], P('tp'), may hold values from -0.75 to 0.75
- query_gain: float32 [64], replicated, may hold values from 1 to 5.5
- key_gain: float32 [64], replicated, may hold values from 1 to 5.5
- context_bias: float32 [16], P('tp'), may hold values from 0.5 to 2
Outputs:
- updated: bfloat16 [2, 16384, 2048], P('dp', 'sp')
All inputs are finite; a program needn't handle non-finite values.
Results may differ from a plain program's by a relative error of at most 0.01405.
The roundings to bfloat16 on the way count: a program that leaves them out, or rounds other values in their place, can miss the bound.
Values may be sent and summed in bfloat16 or wider, within the bound.
A program may use at most 64 MiB of HBM per device.

v0:
```python
import math
import jax
import jax.numpy as jnp
from jax import lax
from jax.sharding import PartitionSpec as P

GRID_W = 64
norm_eps = 1e-06
rope_base = 10000.0


def from_everyone(array, axis):
    size = lax.axis_size(axis)
    return lax.all_to_all(
        jnp.broadcast_to(array[None], (size, *array.shape)), axis, 0, 0, tiled=True
    )


def of_everyone(array, axis):
    return from_everyone(array, axis).sum(axis=0)


def laid_out(pieces, dim):
    dims = list(pieces.shape[1:])
    dims[dim] *= pieces.shape[0]
    return jnp.moveaxis(pieces, 0, dim).reshape(dims)


def gathered_copies(array, axis, dim):
    pieces = from_everyone(array, axis)
    return laid_out(pieces, dim)


def cut_along(array, dim, size):
    before, after = (array.shape[:dim], array.shape[dim + 1 :])
    return jnp.moveaxis(array.reshape(*before, size, -1, *after), dim, 0)


def sent_and_summed(array, axis, dim):
    size = lax.axis_size(axis)
    pieces = lax.all_to_all(cut_along(array, dim, size), axis, 0, 0, tiled=True)
    return jnp.sum(pieces.astype(jnp.float32), axis=0)


def rotary_tables(position, grid_width, head_dim):
    grid_row = (position // grid_width).astype(jnp.float32)
    grid_col = (position % grid_width).astype(jnp.float32)
    quarter = head_dim // 4
    inverse = rope_base ** (-jnp.arange(quarter, dtype=jnp.float32) / quarter)
    angles = jnp.concatenate([grid_row[:, None] * inverse, grid_col[:, None] * inverse], axis=-1)
    return (jnp.cos(angles), jnp.sin(angles))


def head_norm(values, gain_row):
    return (
        values * lax.rsqrt(jnp.mean(values * values, axis=-1, keepdims=True) + norm_eps) * gain_row
    )


def rotate(values, cosine, sine_part):
    half_dim = values.shape[-1] // 2
    first_half = values[..., :half_dim]
    second_half = values[..., half_dim:]
    cos_rows = cosine[:, None, :]
    sin_rows = sine_part[:, None, :]
    return jnp.concatenate(
        [
            first_half * cos_rows - second_half * sin_rows,
            second_half * cos_rows + first_half * sin_rows,
        ],
        axis=-1,
    )


def modulated(tokens, gain_row, shift_row, scale_row):
    floats = tokens.astype(jnp.float32)
    normal = floats * lax.rsqrt(jnp.mean(floats * floats, axis=-1, keepdims=True) + norm_eps)
    return (normal * gain_row * (1.0 + scale_row) + shift_row).astype(jnp.bfloat16)


def on_device(
    latent,
    condition,
    context,
    context_code,
    shift_weight,
    scale_weight,
    gate_weight,
    norm_gain,
    query_weight,
    key_weight,
    value_weight,
    output_weight,
    query_gain,
    key_gain,
    context_bias,
):
    head_dim = query_gain.shape[0]
    tp_size = lax.axis_size("tp")
    activated = jax.nn.silu(condition[0].astype(jnp.float32)).astype(jnp.bfloat16)
    context_act = jax.nn.silu(context_code.astype(jnp.float32)).astype(jnp.bfloat16)
    partial_mod = jnp.stack(
        [
            jnp.dot(activated, shift_weight, preferred_element_type=jnp.float32),
            jnp.dot(activated, scale_weight, preferred_element_type=jnp.float32),
            jnp.dot(activated, gate_weight, preferred_element_type=jnp.float32),
            jnp.dot(context_act, shift_weight, preferred_element_type=jnp.float32),
            jnp.dot(context_act, scale_weight, preferred_element_type=jnp.float32),
        ]
    )
    summed = of_everyone(partial_mod, "sp")
    vectors = gathered_copies(summed, "tp", 1)
    normed = modulated(latent[0], norm_gain, vectors[0], vectors[1])
    query_cols = query_weight.shape[1]
    key_cols = key_weight.shape[1]
    projected = jnp.concatenate(
        [
            jnp.dot(normed, query_weight, preferred_element_type=jnp.float32),
            jnp.dot(normed, key_weight, preferred_element_type=jnp.float32),
            jnp.dot(normed, value_weight, preferred_element_type=jnp.float32),
        ],
        axis=1,
    )
    seq_rows = projected.shape[0]
    position = lax.axis_index("sp") * seq_rows + jnp.arange(seq_rows, dtype=jnp.int32)
    cosine, sine_part = rotary_tables(position, GRID_W, head_dim)
    group_size = query_cols // head_dim
    queries = projected[:, :query_cols].reshape(seq_rows, group_size, head_dim)
    queries = rotate(head_norm(queries, query_gain), cosine, sine_part).astype(jnp.bfloat16)
    latent_keys = projected[:, query_cols : query_cols + key_cols].reshape(seq_rows, 1, head_dim)
    latent_keys = rotate(head_norm(latent_keys, key_gain), cosine, sine_part).astype(jnp.bfloat16)
    latent_values = projected[:, query_cols + key_cols :].astype(jnp.bfloat16)
    key_value = jnp.concatenate([latent_keys.reshape(seq_rows, head_dim), latent_values], axis=1)
    context_normed = modulated(context[0], norm_gain, vectors[3], vectors[4])
    context_keys = head_norm(
        jnp.dot(context_normed, key_weight, preferred_element_type=jnp.float32), key_gain
    )
    context_values = jnp.dot(context_normed, value_weight, preferred_element_type=jnp.float32)
    context_kv = gathered_copies(
        jnp.concatenate(
            [context_keys.astype(jnp.bfloat16), context_values.astype(jnp.bfloat16)], axis=1
        ),
        "sp",
        0,
    )
    score_scale = head_dim ** (-0.5)
    query_rows = queries.transpose(1, 0, 2).reshape(group_size * seq_rows, head_dim)
    bias_rows = jnp.repeat(context_bias, seq_rows)
    context_scores = jnp.dot(
        query_rows, context_kv[:, :head_dim].T, preferred_element_type=jnp.float32
    )
    context_scores = context_scores * score_scale + bias_rows[:, None]
    first_max = context_scores.max(axis=1)
    context_exp = jnp.exp(context_scores - first_max[:, None])
    start_state = (
        first_max,
        context_exp.sum(axis=1),
        jnp.dot(
            context_exp.astype(jnp.bfloat16),
            context_kv[:, head_dim:],
            preferred_element_type=jnp.float32,
        ),
    )
    arrived = lax.all_gather(key_value, "sp", axis=0, tiled=True)
    arrived_rows = arrived.shape[0]
    block_rows = math.gcd(arrived_rows, 1024)
    blocks = arrived.reshape(arrived_rows // block_rows, block_rows, 2 * head_dim)

    def absorb_block(state_now, pair_block):
        old_max, old_total, old_accum = state_now
        scores = (
            jnp.dot(query_rows, pair_block[:, :head_dim].T, preferred_element_type=jnp.float32)
            * score_scale
        )
        new_max = jnp.maximum(old_max, scores.max(axis=1))
        factor = jnp.exp(old_max - new_max)
        weights = jnp.exp(scores - new_max[:, None])
        new_accum = old_accum * factor[:, None] + jnp.dot(
            weights.astype(jnp.bfloat16),
            pair_block[:, head_dim:],
            preferred_element_type=jnp.float32,
        )
        return ((new_max, old_total * factor + weights.sum(axis=1), new_accum), None)

    final_state, unused = lax.scan(absorb_block, start_state, blocks)
    row_max, totals, accum = final_state
    attended = (accum / totals[:, None]).astype(jnp.bfloat16)
    attended = (
        attended.reshape(group_size, seq_rows, head_dim)
        .transpose(1, 0, 2)
        .reshape(seq_rows, query_cols)
    )
    own_rows = seq_rows // tp_size
    mixed = sent_and_summed(
        jnp.dot(attended, output_weight, preferred_element_type=jnp.float32).astype(jnp.bfloat16),
        "tp",
        0,
    )
    own_latent = lax.dynamic_slice_in_dim(latent[0], lax.axis_index("tp") * own_rows, own_rows, 0)
    updated = (own_latent.astype(jnp.float32) + vectors[2] * mixed).astype(jnp.bfloat16)
    whole = gathered_copies(updated, "tp", 0)
    return whole[None]


def solution(mesh):
    return jax.shard_map(
        on_device,
        mesh=mesh,
        in_specs=(
            P("dp", "sp", None),
            P("dp", "sp"),
            P("dp", "sp", None),
            P("sp"),
            P("sp", "tp"),
            P("sp", "tp"),
            P("sp", "tp"),
            P(),
            P(None, "tp"),
            P(None, "tp"),
            P(None, "tp"),
            P("tp", None),
            P(),
            P(),
            P("tp"),
        ),
        out_specs=P("dp", "sp", None),
        check_vma=False,
    )
```

profile of v0, /device:TPU:8, one launch (start us, length us, event | category | flops | bytes accessed | tf_op | source)
XLA Modules:
  0.0 259.9 jit_solution(298645395595733858)
XLA Ops:
  6.5 1.0 fusion.59
  11.3 1.1 broadcast_in_dim.12
  12.4 16.6 %all-to-all-start = ((f32[64,5,512]{2,1,0:T(8,128)}), f32[64,5,512]{2,1,0:T(8,128)S(1)}, u32[]{:S(2)}, u32[]{:S(2)}) async-start(f32[64,5,512]{2,1,0:T(8,128)} %broadcast_in_dim.12), calls=%async_computation | async-start | bytes 2097152 | tf_op jit(solution)/shard_map/all_to_all | solution.py:14
  29.0 2.1 fusion.16
  31.2 27.1 %all-to-all-done = f32[64,5,512]{2,1,0:T(8,128)S(1)} async-done(((f32[64,5,512]{2,1,0:T(8,128)}), f32[64,5,512]{2,1,0:T(8,128)S(1)}, u32[]{:S(2)}, u32[]{:S(2)}) %all-to-all-start) | async-done | bytes 655392 | tf_op jit(solution)/shard_map/all_to_all | solution.py:14
  59.0 4.3 %all-to-all-start.1 = ((f32[4,5,512]{2,1,0:T(8,128)}), f32[4,5,512]{2,1,0:T(8,128)S(1)}, u32[]{:S(2)}, u32[]{:S(2)}) async-start(f32[4,5,512]{2,1,0:T(8,128)} %broadcast_in_dim.13), calls=%async_computation.1 | async-start | bytes 131072 | tf_op jit(solution)/shard_map/all_to_all | solution.py:14
  63.3 1.3 add_rsqrt_fusion.2
  64.6 4.3 %all-to-all-done.1 = f32[4,5,512]{2,1,0:T(8,128)S(1)} async-done(((f32[4,5,512]{2,1,0:T(8,128)}), f32[4,5,512]{2,1,0:T(8,128)S(1)}, u32[]{:S(2)}, u32[]{:S(2)}) %all-to-all-start.1) | async-done | bytes 40992 | tf_op jit(solution)/shard_map/all_to_all | solution.py:14
  69.5 1.6 convolution_convert_fusion.1
  71.2 1.3 multiply_reduce_fusion.2
  74.8 1.4 copy.33
  76.5 1.1 multiply_reduce_fusion.3
  78.3 1.2 convolution_convert_fusion.2
  80.3 7.0 %all-to-all-start.2 = ((bf16[64,16,128]{2,1,0:T(8,128)(2,1)}), bf16[64,16,128]{2,1,0:T(8,128)(2,1)S(1)}, u32[]{:S(2)}, u32[]{:S(2)}) async-start(bf16[64,16,128]{2,1,0:T(8,128)(2,1)} %broadcast_in_dim.14), calls=%async_computation.2 | async-start | bytes 524288 | tf_op jit(solution)/shard_map/all_to_all | solution.py:14
  87.3 2.0 multiply_reduce_fusion.1
  89.7 10.9 %all-to-all-done.2 = bf16[64,16,128]{2,1,0:T(8,128)(2,1)S(1)} async-done(((bf16[64,16,128]{2,1,0:T(8,128)(2,1)}), bf16[64,16,128]{2,1,0:T(8,128)(2,1)S(1)}, u32[]{:S(2)}, u32[]{:S(2)}) %all-to-all-start.2) | async-done | bytes 262176 | tf_op jit(solution)/shard_map/all_to_all | solution.py:14
  102.1 1.0 fusion.25
  103.1 57.5 %all-gather.2.cloned.1.call-done = bf16[16384,128]{0,1:T(8,128)(2,1)} async-done(((bf16[256,128]{0,1:T(8,128)(2,1)}), bf16[16384,128]{0,1:T(8,128)(2,1)}) %all-gather.2.cloned.1.call-update) | async-done | bytes 4194320 | tf_op jit(solution)/shard_map/all_gather | solution.py:164
  160.6 6.4 %copy.38 = bf16[16384,128]{1,0:T(8,128)(2,1)} copy(bf16[16384,128]{0,1:T(8,128)(2,1)} %all-gather.2.cloned.1.call-done) | data formatting | bytes 8388608 | tf_op jit(solution)/shard_map/while | solution.py:185
  167.0 54.7 %while.14 = (s32[]{:T(128)}, f32[1024]{0:T(1024)S(1)}, f32[1024]{0:T(1024)S(1)}, f32[1024,64]{0,1:T(8,128)S(1)}, bf16[16,1024,128]{2,1,0:T(8,128)(2,1)}, /*index=5*/bf16[1024,64]{1,0:T(8,128)(2,1)S(1)}, s32[]{:T(128)}) while((s32[]{:T(128)}, f32[1024]{0:T(1024)S(1)}, f32[1024]{0:T(1024)S(1)}, f32[1024,64]{0,1:T(8,128)S(1)}, ...), condition=%wide.region_11.12_spmd, body=%wide.region_8.11_spmd.sunk | while | flops 276957184 | bytes 14352473 | solution.py:185
  170.4 1.0 dynamic-slice_bitcast_fusion.2
  173.8 1.0 dynamic-slice_bitcast_fusion.2
  177.2 1.0 dynamic-slice_bitcast_fusion.2
  184.1 1.0 dynamic-slice_bitcast_fusion.2
  187.5 1.0 dynamic-slice_bitcast_fusion.2
  190.9 1.0 dynamic-slice_bitcast_fusion.2
  194.3 1.0 dynamic-slice_bitcast_fusion.2
  197.8 1.0 dynamic-slice_bitcast_fusion.2
  221.9 1.4 convolution_convert_fusion
  223.3 4.2 %all-to-all-start.3 = ((bf16[4,64,2048]{2,1,0:T(8,128)(2,1)}), bf16[4,64,2048]{2,1,0:T(8,128)(2,1)S(1)}, u32[]{:S(2)}, u32[]{:S(2)}) async-start(bf16[4,64,2048]{2,1,0:T(8,128)(2,1)} %bitcast.36), calls=%async_computation.3 | async-start | bytes 2097152 | tf_op jit(solution)/shard_map/all_to_all | solution.py:41
  227.5 10.9 %all-to-all-done.3 = bf16[4,64,2048]{2,1,0:T(8,128)(2,1)S(1)} async-done(((bf16[4,64,2048]{2,1,0:T(8,128)(2,1)}), bf16[4,64,2048]{2,1,0:T(8,128)(2,1)S(1)}, u32[]{:S(2)}, u32[]{:S(2)}) %all-to-all-start.3) | async-done | bytes 1048608 | tf_op jit(solution)/shard_map/all_to_all | solution.py:41
  238.8 13.3 %all_to_all.25 = bf16[4,64,2048]{2,1,0:T(8,128)(2,1)S(1)} all-to-all(bf16[4,64,2048]{2,1,0:T(8,128)(2,1)S(1)} %broadcast_in_dim.17), channel_id=1, replica_groups=mesh['sp'=64,'tp'=4,'dp'=2] {'tp'}, dimensions={0} | all-to-all | bytes 2097152 | tf_op jit(solution)/shard_map/all_to_all | solution.py:14
  (163 shorter events, 58.7 us)
Async XLA Ops:
  6.5 215.3 %copy-start = (bf16[256,2048]{1,0:T(8,128)(2,1)S(1)}, bf16[256,2048]{1,0:T(8,128)(2,1)}, u32[]{:S(2)}) copy-start(bf16[256,2048]{1,0:T(8,128)(2,1)} %param.28) | copy-start | bytes 3145732
  6.5 63.0 %copy-start.1 = (bf16[1,256,2048]{2,1,0:T(8,128)(2,1)S(1)}, bf16[1,256,2048]{2,1,0:T(8,128)(2,1)}, u32[]{:S(2)}) copy-start(bf16[1,256,2048]{2,1,0:T(8,128)(2,1)} %param.17) | copy-start | bytes 3145732
  11.2 59.9 %copy-start.4 = (bf16[2048,64]{0,1:T(8,128)(2,1)S(1)}, bf16[2048,64]{0,1:T(8,128)(2,1)}, u32[]{:S(2)}) copy-start(bf16[2048,64]{0,1:T(8,128)(2,1)} %param.26) | copy-start | bytes 786436
  12.4 45.9 %all-to-all-start = ((f32[64,5,512]{2,1,0:T(8,128)}), f32[64,5,512]{2,1,0:T(8,128)S(1)}, u32[]{:S(2)}, u32[]{:S(2)}) async-start(f32[64,5,512]{2,1,0:T(8,128)} %broadcast_in_dim.12), calls=%async_computation | async-start | bytes 2097152 | tf_op jit(solution)/shard_map/all_to_all | solution.py:14
  58.3 16.5 %copy-start.2 = (bf16[2048,256]{1,0:T(8,128)(2,1)S(1)}, bf16[2048,256]{1,0:T(8,128)(2,1)}, u32[]{:S(2)}) copy-start(bf16[2048,256]{1,0:T(8,128)(2,1)} %param.25) | copy-start | bytes 3145732
  59.0 9.9 %all-to-all-start.1 = ((f32[4,5,512]{2,1,0:T(8,128)}), f32[4,5,512]{2,1,0:T(8,128)S(1)}, u32[]{:S(2)}, u32[]{:S(2)}) async-start(f32[4,5,512]{2,1,0:T(8,128)} %broadcast_in_dim.13), calls=%async_computation.1 | async-start | bytes 131072 | tf_op jit(solution)/shard_map/all_to_all | solution.py:14
  63.3 97.3 %all-gather.2.cloned.1.call-start = ((), (), s32[]{:S(2)}) async-start(), calls=%async_computation.5 | async-start | bytes 4259840 | tf_op jit(solution)/shard_map/all_gather | solution.py:164
  69.5 3.9 %copy-start.6 = (f32[1,4,512]{2,0,1:T(1,128)}, f32[1,4,512]{2,0,1:T(1,128)S(1)}, u32[]{:S(2)}) copy-start(f32[1,4,512]{2,0,1:T(1,128)S(1)} %get-tuple-element.93) | copy-start | bytes 24580
  69.5 3.9 %copy-start.7 = (f32[1,4,512]{2,0,1:T(1,128)}, f32[1,4,512]{2,0,1:T(1,128)S(1)}, u32[]{:S(2)}) copy-start(f32[1,4,512]{2,0,1:T(1,128)S(1)} %get-tuple-element.94) | copy-start | bytes 24580
  69.5 6.8 %copy-start.3 = (bf16[1,16,2048]{2,1,0:T(8,128)(2,1)S(1)}, bf16[1,16,2048]{2,1,0:T(8,128)(2,1)}, u32[]{:S(2)}) copy-start(bf16[1,16,2048]{2,1,0:T(8,128)(2,1)} %param.19) | copy-start | bytes 196612
  74.8 14.5 %copy-start.8 = (f32[64]{0:T(128)S(1)}, f32[64]{0:T(128)}, u32[]{:S(2)}) copy-start(f32[64]{0:T(128)} %param.29) | copy-start | bytes 772
  80.3 20.2 %all-to-all-start.2 = ((bf16[64,16,128]{2,1,0:T(8,128)(2,1)}), bf16[64,16,128]{2,1,0:T(8,128)(2,1)S(1)}, u32[]{:S(2)}, u32[]{:S(2)}) async-start(bf16[64,16,128]{2,1,0:T(8,128)(2,1)} %broadcast_in_dim.14), calls=%async_computation.2 | async-start | bytes 524288 | tf_op jit(solution)/shard_map/all_to_all | solution.py:14
  221.7 16.9 %copy-start.5 = (f32[1,4,512]{2,0,1:T(1,128)S(1)}, f32[1,4,512]{2,0,1:T(1,128)}, u32[]{:S(2)}) copy-start(f32[1,4,512]{2,0,1:T(1,128)} %get-tuple-element.90) | copy-start | bytes 24580
  223.3 15.1 %all-to-all-start.3 = ((bf16[4,64,2048]{2,1,0:T(8,128)(2,1)}), bf16[4,64,2048]{2,1,0:T(8,128)(2,1)S(1)}, u32[]{:S(2)}, u32[]{:S(2)}) async-start(bf16[4,64,2048]{2,1,0:T(8,128)(2,1)} %bitcast.36), calls=%async_computation.3 | async-start | bytes 2097152 | tf_op jit(solution)/shard_map/all_to_all | solution.py:41
Sparse Core Ops, SparseCore 0:
  74.2 86.3 all-gather.1
where the time goes:
time: 261 us; the launch traced here: 260 us
  waiting for transfers between devices  111 us (43%)
  matrix products  41.4 us (16%)
  starting transfers between devices  32.1 us (12%)
  local copies, waits for them, and re-layouts  28 us (11%)
  other arithmetic  20 us (8%)
  between operations  13.7 us (5%)
  blocking collectives  13.3 us (5%)
    all_gather x1, waiting for transfers between devices, on_device(): arrived = lax.all_gather(key_value, 'sp', axis=0, tiled=True)  57.5 us
    all_to_all x3, waiting for transfers between devices, from_everyone(): lax.all_to_all(jnp.broadcast_to(array[None], (size, *array.shape)), axis,...  42.3 us
    all_to_all x3, starting transfers between devices, from_everyone(): lax.all_to_all(jnp.broadcast_to(array[None], (size, *array.shape)), axis,...  27.8 us
    squeeze x16, local copies, waits for them, and re-layouts, on_device(): final_state, unused = lax.scan(absorb_block, start_state, blocks)  15.5 us
    dot_general x16, matrix products, absorb_block(): jnp.dot(weights.astype(jnp.bfloat16), pair_block[:, head_dim:], preferred...  14.9 us
    all_to_all x1, blocking collectives, from_everyone(): lax.all_to_all(jnp.broadcast_to(array[None], (size, *array.shape)), axis,...  13.3 us
    reduce_sum x16, other arithmetic, absorb_block(): weights.sum(axis=1)  11.7 us
    dot_general x16, matrix products, absorb_block(): jnp.dot(query_rows, pair_block[:, :head_dim].T, preferred_element_type=jn...  11.5 us
  transfers between devices with their start and end apart: 5, of which 5 were waited for; matrix products, arithmetic and copies ran while one was open for 6% of the time, Pallas kernels for 0%

commit v1 on v0

--- a/solution.py
+++ b/solution.py
@@ -161,7 +161,9 @@
             preferred_element_type=jnp.float32,
         ),
     )
-    arrived = lax.all_gather(key_value, "sp", axis=0, tiled=True)
+    arrived = jnp.concatenate(
+        lax.all_to_all(jnp.stack([key_value] * lax.axis_size("sp")), "sp", 0, 0), axis=0
+    )
     arrived_rows = arrived.shape[0]
     block_rows = math.gcd(arrived_rows, 1024)
     blocks = arrived.reshape(arrived_rows // block_rows, block_rows, 2 * head_dim)

time: 261 us -> 306 us (1.17)
  the two profiles are of different devices: /device:TPU:8 before, /device:TPU:112 now
where the time goes in v1:
time: 306 us; the launch traced here: 305 us
  waiting for transfers between devices  167 us (55%)
  matrix products  40.4 us (13%)
  starting transfers between devices  39.4 us (13%)
  local copies, waits for them, and re-layouts  24.1 us (8%)
  other arithmetic  18.8 us (6%)
  blocking collectives  13.3 us (4%)
    all_to_all x1, waiting for transfers between devices, on_device(): lax.all_to_all(jnp.stack([key_value] * lax.axis_size('sp')), 'sp', 0, 0)  114 us
    all_to_all x3, waiting for transfers between devices, from_everyone(): lax.all_to_all(jnp.broadcast_to(array[None], (size, *array.shape)), axis,...  39.3 us
    all_to_all x3, starting transfers between devices, from_everyone(): lax.all_to_all(jnp.broadcast_to(array[None], (size, *array.shape)), axis,...  27.1 us
    squeeze x16, local copies, waits for them, and re-layouts, on_device(): final_state, unused = lax.scan(absorb_block, start_state, blocks)  15.5 us
    dot_general x16, matrix products, absorb_block(): jnp.dot(weights.astype(jnp.bfloat16), pair_block[:, head_dim:], preferred...  14.9 us
    all_to_all x1, waiting for transfers between devices, sent_and_summed(): pieces = lax.all_to_all(cut_along(array, dim, size), axis, 0, 0, tiled=True)  13.5 us
    all_to_all x1, blocking collectives, from_everyone(): lax.all_to_all(jnp.broadcast_to(array[None], (size, *array.shape)), axis,...  13.3 us
    reduce_sum x16, other arithmetic, absorb_block(): weights.sum(axis=1)  11.7 us
  transfers between devices with their start and end apart: 5, of which 5 were waited for; matrix products, arithmetic and copies ran while one was open for 4% of the time, Pallas kernels for 0%

profile of v1, /device:TPU:112, one launch (start us, length us, event | category | flops | bytes accessed | tf_op | source)
XLA Modules:
  0.0 304.5 jit_solution(18385532755915616692)
XLA Ops:
  0.0 1.1 fusion.59
  4.7 1.1 broadcast_in_dim.12
  5.8 15.1 %all-to-all-start = ((f32[64,5,512]{2,1,0:T(8,128)}), f32[64,5,512]{2,1,0:T(8,128)S(1)}, u32[]{:S(2)}, u32[]{:S(2)}) async-start(f32[64,5,512]{2,1,0:T(8,128)} %broadcast_in_dim.12), calls=%async_computation | async-start | bytes 2097152 | tf_op jit(solution)/shard_map/all_to_all | solution.py:14
  21.0 1.5 fusion.40
  22.6 1.5 fusion.16
  24.7 24.9 %all-to-all-done = f32[64,5,512]{2,1,0:T(8,128)S(1)} async-done(((f32[64,5,512]{2,1,0:T(8,128)}), f32[64,5,512]{2,1,0:T(8,128)S(1)}, u32[]{:S(2)}, u32[]{:S(2)}) %all-to-all-start) | async-done | bytes 655392 | tf_op jit(solution)/shard_map/all_to_all | solution.py:14
  50.3 4.3 %all-to-all-start.1 = ((f32[4,5,512]{2,1,0:T(8,128)}), f32[4,5,512]{2,1,0:T(8,128)S(1)}, u32[]{:S(2)}, u32[]{:S(2)}) async-start(f32[4,5,512]{2,1,0:T(8,128)} %broadcast_in_dim.13), calls=%async_computation.1 | async-start | bytes 131072 | tf_op jit(solution)/shard_map/all_to_all | solution.py:14
  55.3 5.0 %all-to-all-done.1 = f32[4,5,512]{2,1,0:T(8,128)S(1)} async-done(((f32[4,5,512]{2,1,0:T(8,128)}), f32[4,5,512]{2,1,0:T(8,128)S(1)}, u32[]{:S(2)}, u32[]{:S(2)}) %all-to-all-start.1) | async-done | bytes 40992 | tf_op jit(solution)/shard_map/all_to_all | solution.py:14
  60.3 1.2 convolution_convert_fusion.2
  61.5 1.1 multiply_reduce_fusion.3
  62.6 1.3 multiply_reduce_fusion.2
  65.5 7.7 %all-to-all-start.2 = ((bf16[64,16,128]{2,1,0:T(8,128)(2,1)}), bf16[64,16,128]{2,1,0:T(8,128)(2,1)S(1)}, u32[]{:S(2)}, u32[]{:S(2)}) async-start(bf16[64,16,128]{2,1,0:T(8,128)(2,1)} %broadcast_in_dim.14), calls=%async_computation.2 | async-start | bytes 524288 | tf_op jit(solution)/shard_map/all_to_all | solution.py:14
  74.2 9.5 %all-to-all-done.2 = bf16[64,16,128]{2,1,0:T(8,128)(2,1)S(1)} async-done(((bf16[64,16,128]{2,1,0:T(8,128)(2,1)}), bf16[64,16,128]{2,1,0:T(8,128)(2,1)S(1)}, u32[]{:S(2)}, u32[]{:S(2)}) %all-to-all-start.2) | async-done | bytes 262176 | tf_op jit(solution)/shard_map/all_to_all | solution.py:14
  83.6 3.0 stack.20
  86.6 8.8 %all-to-all-start.3 = ((bf16[64,256,128]{2,1,0:T(8,128)(2,1)}), bf16[64,256,128]{2,1,0:T(8,128)(2,1)}, u32[]{:S(2)}, u32[]{:S(2)}) async-start(bf16[64,256,128]{2,1,0:T(8,128)(2,1)} %stack.20), calls=%async_computation.3 | async-start | bytes 8388608 | tf_op jit(solution)/shard_map/all_to_all | solution.py:165
  95.6 1.4 copy.33
  97.1 1.9 multiply_reduce_fusion.1
  101.0 1.0 fusion.25
  102.0 114.5 %all-to-all-done.3 = bf16[64,256,128]{2,1,0:T(8,128)(2,1)} async-done(((bf16[64,256,128]{2,1,0:T(8,128)(2,1)}), bf16[64,256,128]{2,1,0:T(8,128)(2,1)}, u32[]{:S(2)}, u32[]{:S(2)}) %all-to-all-start.3) | async-done | bytes 4194336 | tf_op jit(solution)/shard_map/all_to_all | solution.py:165
  216.5 54.7 %while.14 = (s32[]{:T(128)}, f32[1024]{0:T(1024)S(1)}, f32[1024]{0:T(1024)S(1)}, f32[1024,64]{0,1:T(8,128)S(1)}, bf16[16,1024,128]{2,1,0:T(8,128)(2,1)}, /*index=5*/bf16[1024,64]{1,0:T(8,128)(2,1)S(1)}, s32[]{:T(128)}) while((s32[]{:T(128)}, f32[1024]{0:T(1024)S(1)}, f32[1024]{0:T(1024)S(1)}, f32[1024,64]{0,1:T(8,128)S(1)}, ...), condition=%wide.region_11.12_spmd, body=%wide.region_8.11_spmd.sunk | while | flops 276957184 | bytes 14352473 | solution.py:187
  219.9 1.0 dynamic-slice_bitcast_fusion.2
  223.4 1.0 dynamic-slice_bitcast_fusion.2
  226.8 1.0 dynamic-slice_bitcast_fusion.2
  230.2 1.0 dynamic-slice_bitcast_fusion.2
  233.6 1.0 dynamic-slice_bitcast_fusion.2
  237.0 1.0 dynamic-slice_bitcast_fusion.2
  240.4 1.0 dynamic-slice_bitcast_fusion.2
  243.9 1.0 dynamic-slice_bitcast_fusion.2
  271.4 1.4 convolution_convert_fusion
  272.8 3.5 %all-to-all-start.4 = ((bf16[4,64,2048]{2,1,0:T(8,128)(2,1)}), bf16[4,64,2048]{2,1,0:T(8,128)(2,1)S(1)}, u32[]{:S(2)}, u32[]{:S(2)}) async-start(bf16[4,64,2048]{2,1,0:T(8,128)(2,1)} %bitcast.36), calls=%async_computation.4 | async-start | bytes 2097152 | tf_op jit(solution)/shard_map/all_to_all | solution.py:41
  276.3 13.5 %all-to-all-done.4 = bf16[4,64,2048]{2,1,0:T(8,128)(2,1)S(1)} async-done(((bf16[4,64,2048]{2,1,0:T(8,128)(2,1)}), bf16[4,64,2048]{2,1,0:T(8,128)(2,1)S(1)}, u32[]{:S(2)}, u32[]{:S(2)}) %all-to-all-start.4) | async-done | bytes 1048608 | tf_op jit(solution)/shard_map/all_to_all | solution.py:41
  290.2 13.3 %all_to_all.30 = bf16[4,64,2048]{2,1,0:T(8,128)(2,1)S(1)} all-to-all(bf16[4,64,2048]{2,1,0:T(8,128)(2,1)S(1)} %broadcast_in_dim.17), channel_id=1, replica_groups=mesh['sp'=64,'tp'=4,'dp'=2] {'tp'}, dimensions={0} | all-to-all | bytes 2097152 | tf_op jit(solution)/shard_map/all_to_all | solution.py:14
  (169 shorter events, 57.9 us)
Async XLA Ops:
  0.0 271.4 %copy-start = (bf16[256,2048]{1,0:T(8,128)(2,1)S(1)}, bf16[256,2048]{1,0:T(8,128)(2,1)}, u32[]{:S(2)}) copy-start(bf16[256,2048]{1,0:T(8,128)(2,1)} %param.28) | copy-start | bytes 3145732
  0.0 60.3 %copy-start.3 = (bf16[1,16,2048]{2,1,0:T(8,128)(2,1)S(1)}, bf16[1,16,2048]{2,1,0:T(8,128)(2,1)}, u32[]{:S(2)}) copy-start(bf16[1,16,2048]{2,1,0:T(8,128)(2,1)} %param.19) | copy-start | bytes 196612
  0.0 62.6 %copy-start.1 = (bf16[1,256,2048]{2,1,0:T(8,128)(2,1)S(1)}, bf16[1,256,2048]{2,1,0:T(8,128)(2,1)}, u32[]{:S(2)}) copy-start(bf16[1,256,2048]{2,1,0:T(8,128)(2,1)} %param.17) | copy-start | bytes 3145732
  0.0 61.5 %copy-start.4 = (bf16[2048,64]{0,1:T(8,128)(2,1)S(1)}, bf16[2048,64]{0,1:T(8,128)(2,1)}, u32[]{:S(2)}) copy-start(bf16[2048,64]{0,1:T(8,128)(2,1)} %param.26) | copy-start | bytes 786436
  5.8 43.7 %all-to-all-start = ((f32[64,5,512]{2,1,0:T(8,128)}), f32[64,5,512]{2,1,0:T(8,128)S(1)}, u32[]{:S(2)}, u32[]{:S(2)}) async-start(f32[64,5,512]{2,1,0:T(8,128)} %broadcast_in_dim.12), calls=%async_computation | async-start | bytes 2097152 | tf_op jit(solution)/shard_map/all_to_all | solution.py:14
  49.7 23.5 %copy-start.7 = (f32[64]{0:T(128)S(1)}, f32[64]{0:T(128)}, u32[]{:S(2)}) copy-start(f32[64]{0:T(128)} %param.30) | copy-start | bytes 772
  49.7 23.7 %copy-start.5 = (bf16[2048,64]{0,1:T(8,128)(2,1)S(1)}, bf16[2048,64]{0,1:T(8,128)(2,1)}, u32[]{:S(2)}) copy-start(bf16[2048,64]{0,1:T(8,128)(2,1)} %param.27) | copy-start | bytes 786436
  49.7 23.7 %copy-start.6 = (f32[2048]{0:T(1024)S(1)}, f32[2048]{0:T(1024)}, u32[]{:S(2)}) copy-start(f32[2048]{0:T(1024)} %param.24) | copy-start | bytes 24580
  49.7 23.7 %copy-start.8 = (f32[256]{0:T(256)S(1)}, f32[256]{0:T(256)}, u32[]{:S(2)}) copy-start(f32[256]{0:T(256)} %add_rsqrt_fusion.2) | copy-start | bytes 3076
  50.3 9.9 %all-to-all-start.1 = ((f32[4,5,512]{2,1,0:T(8,128)}), f32[4,5,512]{2,1,0:T(8,128)S(1)}, u32[]{:S(2)}, u32[]{:S(2)}) async-start(f32[4,5,512]{2,1,0:T(8,128)} %broadcast_in_dim.13), calls=%async_computation.1 | async-start | bytes 131072 | tf_op jit(solution)/shard_map/all_to_all | solution.py:14
  65.5 18.1 %all-to-all-start.2 = ((bf16[64,16,128]{2,1,0:T(8,128)(2,1)}), bf16[64,16,128]{2,1,0:T(8,128)(2,1)S(1)}, u32[]{:S(2)}, u32[]{:S(2)}) async-start(bf16[64,16,128]{2,1,0:T(8,128)(2,1)} %broadcast_in_dim.14), calls=%async_computation.2 | async-start | bytes 524288 | tf_op jit(solution)/shard_map/all_to_all | solution.py:14
  86.6 8.9 %copy-start.11 = (f32[4]{0:T(128)S(1)}, f32[4]{0:T(128)}, u32[]{:S(2)}) copy-start(f32[4]{0:T(128)} %param.31) | copy-start | bytes 52
  86.6 9.0 %copy-start.2 = (bf16[2048,256]{1,0:T(8,128)(2,1)S(1)}, bf16[2048,256]{1,0:T(8,128)(2,1)}, u32[]{:S(2)}) copy-start(bf16[2048,256]{1,0:T(8,128)(2,1)} %param.25) | copy-start | bytes 3145732
  86.6 10.5 %copy-start.9 = (f32[256]{0:T(256)S(1)}, f32[256]{0:T(256)}, u32[]{:S(2)}) copy-start(f32[256]{0:T(256)} %add_rsqrt_fusion.2) | copy-start | bytes 3076
  86.6 129.9 %all-to-all-start.3 = ((bf16[64,256,128]{2,1,0:T(8,128)(2,1)}), bf16[64,256,128]{2,1,0:T(8,128)(2,1)}, u32[]{:S(2)}, u32[]{:S(2)}) async-start(bf16[64,256,128]{2,1,0:T(8,128)(2,1)} %stack.20), calls=%async_computation.3 | async-start | bytes 8388608 | tf_op jit(solution)/shard_map/all_to_all | solution.py:165
  95.5 3.6 %copy-start.10 = (f32[64]{0:T(128)S(1)}, f32[64]{0:T(128)}, u32[]{:S(2)}) copy-start(f32[64]{0:T(128)} %param.29) | copy-start | bytes 772
  272.8 17.1 %all-to-all-start.4 = ((bf16[4,64,2048]{2,1,0:T(8,128)(2,1)}), bf16[4,64,2048]{2,1,0:T(8,128)(2,1)S(1)}, u32[]{:S(2)}, u32[]{:S(2)}) async-start(bf16[4,64,2048]{2,1,0:T(8,128)(2,1)} %bitcast.36), calls=%async_computation.4 | async-start | bytes 2097152 | tf_op jit(solution)/shard_map/all_to_all | solution.py:41
